TPU v7x, 32 devices: a whole 2x2x4 slice. The times are simulated.
32 devices in a mesh: sp: 8 (over z, x), tp: 4 (over y, core).
Axes of the slice: x: 2, y: 2, z: 4, core: 2. Of those that a mesh axis runs over, the one named last changes fastest.
Arguments:
- tokens: bfloat16 [4096, 4096], P('sp'), may hold values from -6 to 6
- norm_gain: float32 [4096], replicated, may hold values from 0.1 to 1.9
- w_pool_in: bfloat16 [4096, 2048], P(None, 'tp'), may hold values from -0.09375 to 0.09375
- w_query: bfloat16 [4096, 2048], P(None, 'tp'), may hold values from -0.15625 to 0.15625
- w_key: bfloat16 [4096, 2048], P(None, 'tp'), may hold values from -0.15625 to 0.15625
- w_value: bfloat16 [4096, 2048], P(None, 'tp'), may hold values from -0.09375 to 0.09375
- pool_mix: bfloat16 [32, 64, 64], P('tp'), may hold values from -0.75 to 0.75
- pool_scale: float32 [2048], P('tp'), may hold values from 0.1 to 1.9
- lam: float32 [16], P('tp'), may hold values from 0.3 to 0.8
- head_gain: float32 [128], replicated, may hold values from 0.1 to 1.9
- pool_proj: bfloat16 [2048, 4096], P('tp'), may hold values from -0.125 to 0.125
- attn_proj: bfloat16 [2048, 4096], P('tp'), may hold values from -0.125 to 0.125
Outputs:
- mixed: bfloat16 [4096, 4096], P(('sp', 'tp'))
All inputs are finite; a program needn't handle non-finite values.
Results may differ from a plain program's by a relative error of at most 0.015.
Values may be sent and summed in bfloat16 or wider, within the bound.
A program may use at most 128 MiB of HBM per device.

v0:
```python
import jax
import jax.numpy as jnp
from jax import lax
from jax.sharding import PartitionSpec as P

GDIM = 64
HEAD = 64
VDIM = 128
SEGMENT = 64
REACH = 16


eps_norm = 1e-06
neg_big = -1e30
out_scale = 0.8


def passed_along(shard, axis, by):
    devices = lax.axis_size(axis)
    pairs = [(i, i + by) for i in range(devices) if 0 <= i + by < devices]
    return lax.ppermute(shard, axis, pairs)


def normalize(rows_in, gain):
    wide = rows_in.astype(jnp.float32)
    scaled = wide * lax.rsqrt(jnp.mean(wide * wide, axis=-1, keepdims=True) + eps_norm) * gain
    return scaled.astype(jnp.bfloat16)


def pooling(pool_in, rim, pool_mix, pool_scale, group_first, offset):
    count_rows, width = pool_in.shape
    padded = jnp.concatenate([rim, pool_in], 0).astype(jnp.float32)
    channel_group = group_first + jnp.arange(width, dtype=jnp.int32) // GDIM
    window = 2 ** (1 + channel_group % 4)
    total = jnp.zeros((count_rows, width), jnp.float32)
    for back in range(REACH):
        low = REACH - 1 - back
        total = total + jnp.where(back < window[None, :], padded[low : low + count_rows], 0.0)
    position = offset + jnp.arange(count_rows, dtype=jnp.int32)
    count = jnp.minimum(position[:, None] + 1, window[None, :]).astype(jnp.float32)
    pooled = (total / count - pool_in.astype(jnp.float32)).astype(jnp.bfloat16)
    groups = pool_mix.shape[0]
    grouped = jnp.einsum(
        "sgi,gio->sgo",
        pooled.reshape(count_rows, groups, GDIM),
        pool_mix,
        preferred_element_type=jnp.float32,
    )
    return (grouped.reshape(count_rows, width) * pool_scale).astype(jnp.bfloat16)


def attend_block(carry, query, keys, values, key_start, query_start):
    peak, weight_sum, weighted = carry
    key_seg = (key_start + jnp.arange(keys.shape[0], dtype=jnp.int32)) // SEGMENT
    query_seg = (query_start + jnp.arange(query.shape[0], dtype=jnp.int32)) // SEGMENT
    allowed = key_seg[None, :] <= query_seg[:, None]
    scores = jnp.einsum(
        "qhmd,khmd->hmqk", query, keys, preferred_element_type=jnp.float32
    ) * HEAD ** (-0.5)
    masked = jnp.where(allowed, scores, neg_big)
    new_peak = jnp.maximum(peak, jnp.max(masked, axis=-1))
    probs = jnp.where(allowed, jnp.exp(masked - new_peak[..., None]), 0.0)
    shrink = jnp.exp(peak - new_peak)
    weight_sum = weight_sum * shrink + jnp.sum(probs, axis=-1)
    weighted = weighted * shrink[..., None] + jnp.einsum(
        "hmqk,khe->hmqe", probs.astype(jnp.bfloat16), values, preferred_element_type=jnp.float32
    )
    return (new_peak, weight_sum, weighted)


def guarded(carry, key_start, key_count, query, query_start, make_keys):
    heads = query.shape[1]
    last_seg = (query_start + query.shape[0] - 1) // SEGMENT

    def update(carry_now):
        keys, values = make_keys()
        keys = keys.reshape(key_count, heads, 2, HEAD)
        values = values.reshape(key_count, heads, VDIM)
        return attend_block(carry_now, query, keys, values, key_start, query_start)

    return lax.cond(key_start // SEGMENT > last_seg, lambda carry_now: carry_now, update, carry)


def sweep(carry, piece, step_fn):
    count_rows = jax.tree.leaves(piece)[0].shape[0]
    block = 512

    def one(carry_now, index):
        first = index * block
        part = jax.tree.map(lambda array: lax.dynamic_slice_in_dim(array, first, block, 0), piece)
        return (step_fn(carry_now, part, first, block), None)

    carry, unused = lax.scan(one, carry, jnp.arange(count_rows // block, dtype=jnp.int32))
    return carry


def body(
    tokens,
    norm_gain,
    w_pool_in,
    w_query,
    w_key,
    w_value,
    pool_mix,
    pool_scale,
    lam,
    head_gain,
    pool_proj,
    attn_proj,
):
    count_rows = tokens.shape[0]
    offset = lax.axis_index("sp") * count_rows
    normed = normalize(tokens, norm_gain)
    pool_in = jnp.dot(normed, w_pool_in, preferred_element_type=jnp.float32).astype(jnp.bfloat16)
    query = jnp.dot(normed, w_query, preferred_element_type=jnp.float32).astype(jnp.bfloat16)
    heads = w_value.shape[1] // VDIM
    query_heads = query.reshape(count_rows, heads, 2, HEAD)
    rim = passed_along(pool_in[count_rows - (REACH - 1) :], "sp", 1)
    group_first = lax.axis_index("tp") * pool_mix.shape[0]
    pool_out = pooling(pool_in, rim, pool_mix, pool_scale, group_first, offset)
    start_carry = (
        jnp.full((heads, 2, count_rows), neg_big, jnp.float32),
        jnp.zeros((heads, 2, count_rows), jnp.float32),
        jnp.zeros((heads, 2, count_rows, VDIM), jnp.float32),
    )
    keys = jnp.dot(normed, w_key, preferred_element_type=jnp.float32).astype(jnp.bfloat16)
    values = jnp.dot(normed, w_value, preferred_element_type=jnp.float32).astype(jnp.bfloat16)

    def add_keys(carry, piece):

        def step(carry_now, part, part_start, block):
            return guarded(
                carry_now, part_start, block, query_heads, offset, lambda: (part[0], part[1])
            )

        return sweep(carry, piece, step)

    carry = add_keys(
        start_carry,
        (
            lax.all_gather(keys, "sp", axis=0, tiled=True),
            lax.all_gather(values, "sp", axis=0, tiled=True),
        ),
    )
    peak, weight_sum, weighted = carry
    averaged = weighted / weight_sum[..., None]
    blend = averaged[:, 0] - lam[:, None, None] * averaged[:, 1]
    scaled = (
        blend
        * lax.rsqrt(jnp.mean(blend * blend, axis=-1, keepdims=True) + eps_norm)
        * head_gain
        * out_scale
    )
    attn_out = scaled.astype(jnp.bfloat16).transpose(1, 0, 2).reshape(count_rows, heads * VDIM)
    term = jnp.dot(pool_out, pool_proj, preferred_element_type=jnp.float32)
    return lax.psum_scatter(
        (term + jnp.dot(attn_out, attn_proj, preferred_element_type=jnp.float32)).astype(
            jnp.bfloat16
        ),
        "tp",
        scatter_dimension=0,
        tiled=True,
    )


def solution(mesh):
    return jax.shard_map(
        body,
        mesh=mesh,
        in_specs=(
            P("sp", None),
            P(),
            P(None, "tp"),
            P(None, "tp"),
            P(None, "tp"),
            P(None, "tp"),
            P("tp", None, None),
            P("tp"),
            P("tp"),
            P(),
            P("tp", None),
            P("tp", None),
        ),
        out_specs=P(("sp", "tp"), None),
        check_vma=False,
    )
```

profile of v0, /device:TPU:0, one launch (start us, length us, event | category | flops | bytes accessed | tf_op | source)
XLA Modules:
  0.0 318.8 jit_solution(4136527174383341581)
XLA Ops:
  6.5 3.2 %fusion.17 = f32[512]{0:T(512)S(1)} fusion(bf16[512,4096]{1,0:T(8,128)(2,1)} %param.16), kind=kLoop, calls=%fused_computation.36 | loop fusion | flops 6290944 | bytes 4196352 | tf_op jit(solution)/shard_map/reduce_sum | solution.py:26
  9.8 0.2 copy-done.2
  10.0 5.4 %convolution_convert_fusion.2 = bf16[512,512]{1,0:T(8,128)(2,1)} fusion(bf16[4096,512]{1,0:T(8,128)(2,1)} %param.20, bf16[512,4096]{1,0:T(8,128)(2,1)S(1)} %copy-done.2, f32[4096]{0:T(1024)} %param.17, f32[512]{0:T(512)S(1)} %add_rsqrt_fusion.1), kind=kOutput, calls=%fused_computation.42 | convolution fusion | flops 2156134400 | bytes 8931328 | tf_op jit(solution)/shard_map/dot_general | solution.py:126
  15.4 0.0 all-gather.3.cloned.1.call-update
  15.4 0.0 all-gather.5.cloned.1.call-start
  15.5 6.6 %convolution_convert_fusion = bf16[512,512]{1,0:T(8,128)(2,1)} fusion(bf16[4096,512]{1,0:T(8,128)(2,1)} %param.21, bf16[512,4096]{1,0:T(8,128)(2,1)} %param.16, f32[4096]{0:T(1024)S(1)} %copy-done.7, f32[512]{0:T(512)S(1)} %add_rsqrt_fusion.1), kind=kOutput, calls=%fused_computation.40 | convolution fusion | flops 2156134400 | bytes 8931328 | tf_op jit(solution)/shard_map/dot_general | solution.py:127
  22.2 0.0 all-gather.5.cloned.1.call-update
  22.2 0.0 reduce-scatter.2.cloned.1.call-start
  22.2 5.9 %convolution_convert_fusion.3 = bf16[512,512]{1,0:T(8,128)(2,1)S(1)} fusion(bf16[4096,512]{1,0:T(8,128)(2,1)} %param.18, bf16[512,4096]{1,0:T(8,128)(2,1)} %param.16, f32[4096]{0:T(1024)S(1)} %copy-done.7, f32[512]{0:T(512)S(1)} %add_rsqrt_fusion.1), kind=kOutput, calls=%fused_computation.43 | convolution fusion | flops 2156134400 | bytes 8931328 | tf_op jit(solution)/shard_map/dot_general | solution.py:114
  28.2 5.1 %collective-permute-start = (bf16[15,512]{1,0:T(8,128)(2,1)S(1)}, bf16[15,512]{1,0:T(8,128)(2,1)S(1)}, u32[]{:S(2)}, u32[]{:S(2)}) collective-permute-start(bf16[15,512]{1,0:T(8,128)(2,1)S(1)} %slice.76), channel_id=1, source_target_pairs={{0,4},{4,8},{8,12},{12,16},{16,20},{20,24},{24,28},{1,5},{5,9},{9,... | collective-permute-start | bytes 46088 | tf_op jit(solution)/shard_map/ppermute | solution.py:21
  33.5 6.0 %convolution_convert_fusion.1 = bf16[512,512]{0,1:T(8,128)(2,1)S(1)} fusion(bf16[4096,512]{1,0:T(8,128)(2,1)} %param.19, bf16[512,4096]{1,0:T(8,128)(2,1)} %param.16, f32[4096]{0:T(1024)S(1)} %copy-done.7, f32[512]{0:T(512)S(1)} %add_rsqrt_fusion.1), kind=kOutput, calls=%fused_computation.41 | convolution fusion | flops 2156134400 | bytes 8931328 | tf_op jit(solution)/shard_map/dot_general | solution.py:115
  39.5 0.0 collective-permute-done
  39.5 0.1 maximum_convert_fusion
  39.7 0.0 copy-start.4
  39.7 3.2 %fusion.40 = bf16[512,512]{1,0:T(8,128)(2,1)S(1)} fusion(bf16[512,512]{1,0:T(8,128)(2,1)S(1)} %convolution_convert_fusion.3, f32[527,512]{1,0:T(8,128)S(1)} %maximum_convert_fusion, s32[512]{0:T(512)S(1)} %get-tuple-element.394, s32[512]{0:T(512)S(1)} %get-tuple-element.395, pred[512]{0:T(512)(128)(4,1)S(1)} %get-tuple-element.378, ...), kind=kLoop, calls=%fused_computation.86 | loop fusion | flops 9699328 | bytes 17838080 | tf_op jit(solution)/shard_map/convert_element_type | solution.py:41
  43.0 0.2 copy.20
  43.2 0.3 fusion.52
  43.5 0.1 fusion.39
  43.7 7.8 %fusion.53 = f32[512,4096]{1,0:T(8,128)} fusion(bf16[512,512]{0,1:T(8,128)(2,1)S(1)} %fusion.39, bf16[512,4096]{1,0:T(8,128)(2,1)} %param.26), kind=kOutput, calls=%fused_computation.132 | convolution fusion | flops 2147483648 | bytes 13107200 | tf_op jit(solution)/shard_map/dot_general | solution.py:155
  51.5 39.9 %all-gather.3.cloned.1.call-done = bf16[4096,512]{1,0:T(8,128)(2,1)} async-done(((bf16[512,512]{1,0:T(8,128)(2,1)}), bf16[4096,512]{1,0:T(8,128)(2,1)}) %all-gather.3.cloned.1.call-update) | async-done | bytes 4194320 | tf_op jit(solution)/shard_map/all_gather | solution.py:141
  91.5 6.5 %copy.22 = bf16[4096,512]{0,1:T(8,128)(2,1)} copy(bf16[4096,512]{1,0:T(8,128)(2,1)} %all-gather.3.cloned.1.call-done) | data formatting | bytes 8388608 | tf_op jit(solution)/shard_map/while | solution.py:93
  97.9 67.0 %all-gather.5.cloned.1.call-done = bf16[4096,512]{1,0:T(8,128)(2,1)} async-done(((bf16[512,512]{1,0:T(8,128)(2,1)}), bf16[4096,512]{1,0:T(8,128)(2,1)}) %all-gather.5.cloned.1.call-update) | async-done | bytes 4194320 | tf_op jit(solution)/shard_map/all_gather | solution.py:142
  164.9 6.4 %copy.23 = bf16[4096,512]{0,1:T(8,128)(2,1)} copy(bf16[4096,512]{1,0:T(8,128)(2,1)} %all-gather.5.cloned.1.call-done) | data formatting | bytes 8388608 | tf_op jit(solution)/shard_map/while | solution.py:93
  171.4 0.1 broadcast_in_dim.184
  171.5 19.9 %while.17 = (s32[]{:T(128)}, f32[4,2,512]{2,1,0:T(2,128)S(1)}, f32[4,2,512]{2,1,0:T(2,128)S(1)}, f32[4,2,512,128]{3,2,1,0:T(8,128)S(1)}, s32[8]{0:T(128)S(1)}, /...) while((s32[]{:T(128)}, f32[4,2,512]{2,1,0:T(2,128)S(1)}, ...), condition=%wide.region_6.7_spmd, body=%wide.region_1.6_spmd.sunk | while | flops 833904640 | bytes 34349548 | solution.py:93
  171.5 0.6 dynamic_slice.31
  172.8 9.3 %conditional.2 = (f32[4,2,512]{2,1,0:T(2,128)S(1)}, f32[4,2,512]{2,1,0:T(2,128)S(1)}, f32[4,2,512,128]{3,2,1,0:T(8,128)S(1)}) conditional(s32[]{:T(128)} %convert_element_type.102, (s32[]{:T(128)}, s32[]{:T(128)}, pred[]{:T(512)}, bf16[4096,512]{0,1:T(8,128)(2,1)}, bf16[512,4,2,64]{0,3,2,1:T(8,128)(2,1)S(1)}, /*index=5*/f32[4,2,512]{2,1,0:T(2,128)S(1)}, ...), branch_computations={%region_2.4_spmd, %region_5.5_spmd} | conditional | flops 833904640 | bytes 34316348 | solution.py:81
  172.8 0.2 broadcast_compare_fusion
  173.1 1.8 constant_dynamic-slice_fusion
  174.8 1.5 fusion
  176.4 2.1 fusion.2
  178.5 3.6 %multiply_add_fusion = f32[4,2,512,128]{3,2,1,0:T(8,128)S(1)} fusion(f32[4,2,512,128]{3,2,1,0:T(8,128)S(1)} %get-tuple-element.310, bf16[512,4,128,1]{0,2,3,1:T(8,128)(2,1)S(1)} %bitcast.72, f32[4,2,512,512]{3,2,1,0:T(8,128)S(1)} %get-tuple-element.373, f32[4,2,512]{2,1,0:T(2,128)S(1)} %max.5, pred[512,512]{0,1:T(8,128)(4,1)S(1)} %broadcast_compare_fusion, ...), kind=kOutput, calls=%fused_computation.7 | convolution fusion | flops 548405248 | bytes 13402112 | tf_op jit(solution)/shard_map/while/body/eval_jaxpr/cond/branch_0_fun/hmqk,khe->hmqe/dot_general | solution.py:65
  182.1 0.6 dynamic_slice.31
  183.5 0.6 dynamic_slice.31
  184.8 0.6 dynamic_slice.31
  186.1 0.6 dynamic_slice.31
  187.5 0.6 dynamic_slice.31
  188.8 0.6 dynamic_slice.31
  190.1 0.6 dynamic_slice.31
  191.5 0.0 copy-start.5
  191.5 2.1 copy.25
  193.6 2.0 broadcast_divide_fusion
  195.6 0.3 multiply_reduce_fusion
  196.0 0.3 multiply_convert_fusion
  196.3 0.2 copy-done.3
  196.4 7.9 %add_convert_fusion = bf16[512,4096]{1,0:T(8,128)(2,1)} fusion(f32[512,4096]{1,0:T(8,128)} %fusion.53, bf16[512,512]{0,1:T(8,128)(2,1)S(1)} %bitcast.75, bf16[512,4096]{1,0:T(8,128)(2,1)S(1)} %copy-done.3), kind=kOutput, calls=%fused_computation.39 | convolution fusion | flops 2151677952 | bytes 17301504 | tf_op jit(solution)/shard_map/dot_general | solution.py:157
  204.3 0.0 reduce-scatter.2.cloned.1.call-update
  204.4 107.9 %reduce-scatter.2.cloned.1.call-done = bf16[128,4096]{1,0:T(8,128)(2,1)} async-done(((bf16[512,4096]{1,0:T(8,128)(2,1)}), bf16[128,4096]{1,0:T(8,128)(2,1)}) %reduce-scatter.2.cloned.1.call-update) | async-done | bytes 1048592 | tf_op jit(solution)/shard_map/reduce_scatter | solution.py:156
  (54 shorter events, 0.6 us)
Async XLA Ops:
  6.5 36.6 %copy-start = (bf16[8,64,64]{2,1,0:T(8,128)(2,1)S(1)}, bf16[8,64,64]{2,1,0:T(8,128)(2,1)}, u32[]{:S(2)}) copy-start(bf16[8,64,64]{2,1,0:T(8,128)(2,1)} %param.22) | copy-start | bytes 196612
  6.5 84.9 %all-gather.3.cloned.1.call-start = ((), (), s32[]{:S(2)}) async-start(), calls=%async_computation.1 | async-start | bytes 4718592 | tf_op jit(solution)/shard_map/all_gather | solution.py:141
  6.5 3.5 %copy-start.2 = (bf16[512,4096]{1,0:T(8,128)(2,1)S(1)}, bf16[512,4096]{1,0:T(8,128)(2,1)}, u32[]{:S(2)}) copy-start(bf16[512,4096]{1,0:T(8,128)(2,1)} %param.16) | copy-start | bytes 12582916
  10.0 5.5 %copy-start.7 = (f32[4096]{0:T(1024)S(1)}, f32[4096]{0:T(1024)}, u32[]{:S(2)}) copy-start(f32[4096]{0:T(1024)} %param.17) | copy-start | bytes 49156
  15.4 149.5 %all-gather.5.cloned.1.call-start = ((), (), s32[]{:S(2)}) async-start(), calls=%async_computation.2 | async-start | bytes 4718592 | tf_op jit(solution)/shard_map/all_gather | solution.py:142
  22.2 290.1 %reduce-scatter.2.cloned.1.call-start = ((), (), s32[]{:S(2)}) async-start(), calls=%async_computation.3 | async-start | bytes 5242880 | tf_op jit(solution)/shard_map/reduce_scatter | solution.py:156
  28.2 11.4 %collective-permute-start = (bf16[15,512]{1,0:T(8,128)(2,1)S(1)}, bf16[15,512]{1,0:T(8,128)(2,1)S(1)}, u32[]{:S(2)}, u32[]{:S(2)}) collective-permute-start(bf16[15,512]{1,0:T(8,128)(2,1)S(1)} %slice.76), channel_id=1, source_target_pairs={{0,4},{4,8},{8,12},{12,16},{16,20},{20,24},{24,28},{1,5},{5,9},{9,... | collective-permute-start | bytes 46088 | tf_op jit(solution)/shard_map/ppermute | solution.py:21
  39.7 3.8 %copy-start.4 = (f32[512]{0:T(512)S(1)}, f32[512]{0:T(512)}, u32[]{:S(2)}) copy-start(f32[512]{0:T(512)} %param.23) | copy-start | bytes 6148
  191.5 4.2 %copy-start.5 = (f32[4]{0:T(128)S(1)}, f32[4]{0:T(128)}, u32[]{:S(2)}) copy-start(f32[4]{0:T(128)} %param.24) | copy-start | bytes 52
  193.6 2.4 copy-start.6
  193.6 2.8 copy-start.3
  196.4 115.9 %copy-start.1 = (bf16[8,64,64]{2,1,0:T(8,128)(2,1)S(1)}, bf16[8,64,64]{2,1,0:T(8,128)(2,1)}, u32[]{:S(2)}) copy-start(bf16[8,64,64]{2,1,0:T(8,128)(2,1)} %param.22) | copy-start | bytes 196612
Sparse Core Ops, SparseCore 0:
  15.6 75.8 all-gather.2
  93.6 71.3 all-gather.4
  204.5 107.7 reduce-scatter.1
where the time goes:
time: 319 us
  waiting for transfers between devices  215 us (67%)
  matrix products  45.2 us (14%)
  local copies, waits for them, and re-layouts  22.3 us (7%)
  between operations  13.3 us (4%)
  other arithmetic  11.9 us (4%)
  loops' own time  5.96 us (2%)
  starting transfers between devices  5.21 us (2%)
    reduce_scatter x1, waiting for transfers between devices, body(): lax.psum_scatter((term + jnp.dot(attn_out, attn_proj, preferred_element_t...  108 us
    all_gather x1, waiting for transfers between devices, body(): lax.all_gather(values, 'sp', axis=0, tiled=True)  67 us
    all_gather x1, waiting for transfers between devices, body(): lax.all_gather(keys, 'sp', axis=0, tiled=True)  39.9 us
    while x4, local copies, waits for them, and re-layouts, sweep(): lax.scan(one, carry, jnp.arange(count_rows // block, dtype=jnp.int32))  15 us
    dot_general x1, matrix products, body(): jnp.dot(attn_out, attn_proj, preferred_element_type=jnp.float32)  7.91 us
    dot_general x1, matrix products, body(): term = jnp.dot(pool_out, pool_proj, preferred_element_type=jnp.float32)  7.82 us
    dot_general x1, matrix products, body(): jnp.dot(normed, w_value, preferred_element_type=jnp.float32)  6.65 us
  transfers between devices with their start and end apart: 4, of which 3 were waited for; matrix products, arithmetic and copies ran while one was open for 12% of the time, Pallas kernels for 0%

commit v1 on v0

v1 whole, which is shorter than its diff:
```python
import functools

import jax
import jax.numpy as jnp
from jax import lax
from jax.experimental import pallas as pl
from jax.experimental.pallas import tpu as pltpu
from jax.sharding import PartitionSpec as P

GDIM = 64
HEAD = 64
VDIM = 128
SEGMENT = 64
REACH = 16
CHUNK = 256

eps_norm = 1e-06
neg_big = -1e30
out_scale = 0.8
log2_e = 1.4426950408889634


def normalize(rows_in, gain):
    wide = rows_in.astype(jnp.float32)
    scaled = wide * lax.rsqrt(jnp.mean(wide * wide, axis=-1, keepdims=True) + eps_norm) * gain
    return scaled.astype(jnp.bfloat16)


def pool_kernel(x_ref, rim_ref, mix_ref, scale_ref, out_ref):
    rows, width = x_ref.shape
    x = x_ref[...].astype(jnp.float32)
    padded = jnp.concatenate([rim_ref[...].astype(jnp.float32), x], 0)
    group = lax.axis_index("tp") * (width // GDIM) + lax.broadcasted_iota(
        jnp.int32, (1, width), 1
    ) // GDIM
    window = 2 << (group % 4)
    running = padded
    total = jnp.zeros_like(padded)
    for level in range(4):
        running = running + pltpu.roll(running, 1 << level, 0)
        total = jnp.where(group % 4 == level, running, total)
    position = lax.axis_index("sp") * rows + lax.broadcasted_iota(jnp.int32, (rows, 1), 0)
    count = jnp.minimum(position + 1, window).astype(jnp.float32)
    pooled = (total[REACH:] / count - x).astype(jnp.bfloat16)
    for pair in range(width // 128):
        cols = slice(pair * 128, pair * 128 + 128)
        mixed = jnp.dot(pooled[:, cols], mix_ref[pair], preferred_element_type=jnp.float32)
        out_ref[:, cols] = (mixed * scale_ref[:, cols]).astype(jnp.bfloat16)


def pooling(pool_in, rim, pool_mix, pool_scale):
    groups = pool_mix.shape[0]
    pairs = pool_mix.reshape(groups // 2, 2, GDIM, GDIM)
    zero = jnp.zeros_like(pairs[:, 0])
    mix = jnp.concatenate(
        [
            jnp.concatenate([pairs[:, 0], zero], 2),
            jnp.concatenate([zero, pairs[:, 1]], 2),
        ],
        1,
    )
    rows, width = pool_in.shape
    return pl.pallas_call(
        pool_kernel,
        out_shape=jax.ShapeDtypeStruct((rows, width), jnp.bfloat16),
        cost_estimate=pl.CostEstimate(
            flops=rows * width * 256, bytes_accessed=4 * rows * width, transcendentals=0
        ),
        name="pooling",
    )(pool_in, rim, mix, pool_scale.reshape(1, width))


def attend_kernel(lam_ref, q_ref, k_ref, v_ref, gain_ref, out_ref, stacked, peak, total, acc):
    rows = q_ref.shape[0]
    head = pl.program_id(0)
    mine = lax.axis_index("sp")
    query = q_ref[...]
    lane = lax.broadcasted_iota(jnp.int32, query.shape, 1)
    stacked[:rows] = jnp.where(lane < HEAD, query, 0)
    stacked[rows:] = jnp.where(lane < HEAD, 0, query)

    def block(index, first):
        k = k_ref[pl.ds(pl.multiple_of(index * rows, rows), rows), :]
        v = v_ref[index]
        for start in range(0, 2 * rows, CHUNK):
            cols = slice(start, start + CHUNK)
            scores = lax.dot_general(
                k, stacked[cols], (((1,), (1,)), ((), ())), preferred_element_type=jnp.float32
            )
            if first:
                key_seg = lax.broadcasted_iota(jnp.int32, (rows, 1), 0) // SEGMENT
                query_seg = (
                    start % rows + lax.broadcasted_iota(jnp.int32, (1, CHUNK), 1)
                ) // SEGMENT
                scores = jnp.where(key_seg <= query_seg, scores, neg_big)
                top = jnp.max(scores, axis=0, keepdims=True)
            else:
                old = peak[:, cols]
                top = jnp.maximum(old, jnp.max(scores, axis=0, keepdims=True))
                shrink = jnp.exp2(old - top)
            probs = jnp.exp2(scores - top)
            summed = jnp.sum(probs, axis=0, keepdims=True)
            weighted = jnp.dot(v, probs.astype(jnp.bfloat16), preferred_element_type=jnp.float32)
            peak[:, cols] = top
            if first:
                total[:, cols] = summed
                acc[:, cols] = weighted
            else:
                total[:, cols] = total[:, cols] * shrink + summed
                acc[:, cols] = acc[:, cols] * shrink + weighted

    block(mine, True)

    @pl.loop(0, mine)
    def _(index):
        block(index, False)

    averaged = acc[...] / total[...]
    blend = averaged[:, :rows] - lam_ref[head] * averaged[:, rows:]
    scaled = blend * lax.rsqrt(jnp.mean(blend * blend, axis=0, keepdims=True) + eps_norm)
    out_ref[...] = (scaled.T * gain_ref[...] * out_scale).astype(jnp.bfloat16)


def attend(query, keys, values, lam, head_gain):
    rows, width = query.shape
    heads = width // VDIM
    parts, tokens = values.shape[0], keys.shape[0]
    work = rows * tokens * heads
    return pl.pallas_call(
        attend_kernel,
        grid=(heads,),
        in_specs=[
            pl.BlockSpec(memory_space=pltpu.SMEM),
            pl.BlockSpec((rows, VDIM), lambda h: (0, h)),
            pl.BlockSpec((tokens, VDIM), lambda h: (0, h)),
            pl.BlockSpec((parts, VDIM, rows), lambda h: (0, h, 0)),
            pl.BlockSpec((1, VDIM), lambda h: (0, 0)),
        ],
        out_specs=pl.BlockSpec((rows, VDIM), lambda h: (0, h)),
        out_shape=jax.ShapeDtypeStruct((rows, width), jnp.bfloat16),
        scratch_shapes=[
            pltpu.VMEM((2 * rows, VDIM), jnp.bfloat16),
            pltpu.VMEM((1, 2 * rows), jnp.float32),
            pltpu.VMEM((1, 2 * rows), jnp.float32),
            pltpu.VMEM((VDIM, 2 * rows), jnp.float32),
        ],
        cost_estimate=pl.CostEstimate(
            flops=work * 1024, bytes_accessed=4 * tokens * width, transcendentals=2 * work
        ),
        compiler_params=pltpu.CompilerParams(vmem_limit_bytes=48 * 2**20),
        name="attend",
    )(lam, query, keys, values, head_gain.reshape(1, VDIM))


def body(
    tokens,
    norm_gain,
    w_pool_in,
    w_query,
    w_key,
    w_value,
    pool_mix,
    pool_scale,
    lam,
    head_gain,
    pool_proj,
    attn_proj,
):
    count_rows = tokens.shape[0]
    normed = normalize(tokens, norm_gain)
    keys = jnp.dot(normed, w_key, preferred_element_type=jnp.float32).astype(jnp.bfloat16)
    all_keys = lax.all_gather(keys, "sp", axis=0, tiled=True)
    values = lax.dot_general(
        w_value, normed, (((0,), (1,)), ((), ())), preferred_element_type=jnp.float32
    ).astype(jnp.bfloat16)
    all_values = lax.all_gather(values, "sp", axis=0, tiled=False)
    pool_in = jnp.dot(normed, w_pool_in, preferred_element_type=jnp.float32).astype(jnp.bfloat16)
    devices = lax.axis_size("sp")
    rim = lax.ppermute(
        pool_in[count_rows - REACH :], "sp", [(i, i + 1) for i in range(devices - 1)]
    )
    query = (
        jnp.dot(normed, w_query, preferred_element_type=jnp.float32) * (HEAD ** (-0.5) * log2_e)
    ).astype(jnp.bfloat16)
    pool_out = pooling(pool_in, rim, pool_mix, pool_scale)
    attn_out = attend(query, all_keys, all_values, lam, head_gain)
    term = jnp.dot(pool_out, pool_proj, preferred_element_type=jnp.float32)
    return lax.psum_scatter(
        (term + jnp.dot(attn_out, attn_proj, preferred_element_type=jnp.float32)).astype(
            jnp.bfloat16
        ),
        "tp",
        scatter_dimension=0,
        tiled=True,
    )


def solution(mesh):
    return jax.shard_map(
        body,
        mesh=mesh,
        in_specs=(
            P("sp", None),
            P(),
            P(None, "tp"),
            P(None, "tp"),
            P(None, "tp"),
            P(None, "tp"),
            P("tp", None, None),
            P("tp"),
            P("tp"),
            P(),
            P("tp", None),
            P("tp", None),
        ),
        out_specs=P(("sp", "tp"), None),
        check_vma=False,
    )
```

time: 319 us -> 281 us (0.88)
  matrix products: 45.2 us -> 27.2 us
  local copies, waits for them, and re-layouts: 22.3 us -> 9.53 us
  Pallas kernels: 0 us -> 12.5 us
  other arithmetic: 11.9 us -> 3.98 us
  waiting for transfers between devices: 215 us -> 209 us
  loops' own time: 5.96 us -> 0 us
    reduce_scatter x1, waiting for transfers between devices: 108 us -> 89.8 us  [body(): lax.psum_scatter((term + jnp.dot(attn_out, attn_proj, preferred_element_t...]
    while x12 -> x0, local copies, waits for them, and re-layouts: 15 us -> none  [the longest x4 15 us: sweep(): lax.scan(one, carry, jnp.arange(count_rows // block, dtype=jnp.int32))]
    pallas_call x0 -> x2, Pallas kernels: none -> 12.5 us  [the longest x1 9.61 us: attend(): pl.pallas_call(attend_kernel, grid=(heads,), in_specs=[pl.BlockSpec(memor...]
    all_gather x2, waiting for transfers between devices: 107 us -> 119 us  [the longest x1 66.7 us: body(): all_keys = lax.all_gather(keys, 'sp', axis=0, tiled=True)]
    dot_general x4 -> x1, matrix products: 12.1 us -> 5.43 us  [body(): lax.dot_general(w_value, normed, (((0,), (1,)), ((), ())), preferred_elem...]
    dynamic_slice x9 -> x0, local copies, waits for them, and re-layouts: 6.47 us -> none  [the longest x8 4.71 us: sweep(): lax.scan(one, carry, jnp.arange(count_rows // block, dtype=jnp.int32))]
    all_gather x0 -> x1, local copies, waits for them, and re-layouts: none -> 6.47 us  [body(): all_values = lax.all_gather(values, 'sp', axis=0, tiled=False)]
    another operation x9 -> x0, loops' own time: 5.96 us -> none  [the longest x1 5.69 us: sweep(): lax.scan(one, carry, jnp.arange(count_rows // block, dtype=jnp.int32))]
  transfers between devices with their start and end apart: 4 -> 4, of which waited for: 3 -> 3; matrix products, arithmetic and copies ran while one was open for 12% -> 8% of each run, Pallas kernels for 0% -> 1%
where the time goes in v1:
time: 281 us
  waiting for transfers between devices  209 us (74%)
  matrix products  27.2 us (10%)
  between operations  13.3 us (5%)
  Pallas kernels  12.5 us (4%)
  local copies, waits for them, and re-layouts  9.53 us (3%)
  starting transfers between devices  5.39 us (2%)
  other arithmetic  3.98 us (1%)
    reduce_scatter x1, waiting for transfers between devices, body(): lax.psum_scatter((term + jnp.dot(attn_out, attn_proj, preferred_element_t...  89.8 us
    all_gather x1, waiting for transfers between devices, body(): all_keys = lax.all_gather(keys, 'sp', axis=0, tiled=True)  66.7 us
    all_gather x1, waiting for transfers between devices, body(): all_values = lax.all_gather(values, 'sp', axis=0, tiled=False)  52.5 us
    pallas_call x1, Pallas kernels, attend(): pl.pallas_call(attend_kernel, grid=(heads,), in_specs=[pl.BlockSpec(memor...  9.61 us
    dot_general x1, matrix products, body(): jnp.dot(normed, w_key, preferred_element_type=jnp.float32)  6.65 us
    all_gather x1, local copies, waits for them, and re-layouts, body(): all_values = lax.all_gather(values, 'sp', axis=0, tiled=False)  6.47 us
    dot_general x1, matrix products, body(): jnp.dot(normed, w_pool_in, preferred_element_type=jnp.float32)  6.1 us
  transfers between devices with their start and end apart: 4, of which 3 were waited for; matrix products, arithmetic and copies ran while one was open for 8% of the time, Pallas kernels for 1%

profile of v1, /device:TPU:0, one launch (start us, length us, event | category | flops | bytes accessed | tf_op | source)
XLA Modules:
  0.0 281.0 jit_solution(6825725803064119611)
XLA Ops:
  6.5 0.0 all-gather.6.cloned.1.call-start
  6.5 0.0 copy-start.4
  6.5 3.2 %fusion = f32[512]{0:T(512)S(1)} fusion(bf16[512,4096]{1,0:T(8,128)(2,1)} %param.12), kind=kLoop, calls=%fused_computation.2 | loop fusion | flops 6290944 | bytes 4196352 | tf_op jit(solution)/shard_map/reduce_sum | solution.py:25
  9.8 0.2 copy-done.4
  10.0 0.0 copy-start.12
  10.0 5.4 %fusion.4 = bf16[512,512]{0,1:T(8,128)(2,1)} fusion(bf16[4096,512]{1,0:T(8,128)(2,1)} %param.17, bf16[512,4096]{1,0:T(8,128)(2,1)S(1)} %copy-done.4, f32[4096]{0:T(1024)} %param.13, f32[512]{0:T(512)S(1)} %add_rsqrt_fusion), kind=kOutput, calls=%fused_computation.11 | convolution fusion | flops 2156134400 | bytes 8931328 | tf_op jit(solution)/shard_map/dot_general | solution.py:173
  15.4 0.0 all-gather.6.cloned.1.call-update
  15.4 0.0 all-gather.4.cloned.1.call-start
  15.5 0.0 copy-done.12
  15.5 6.6 %convolution_convert_fusion.1 = bf16[512,512]{1,0:T(8,128)(2,1)} fusion(bf16[4096,512]{1,0:T(8,128)(2,1)} %param.16, bf16[512,4096]{1,0:T(8,128)(2,1)} %param.12, f32[4096]{0:T(1024)S(1)} %copy-done.12, f32[512]{0:T(512)S(1)} %add_rsqrt_fusion), kind=kOutput, calls=%fused_computation.9 | convolution fusion | flops 2156134400 | bytes 8931328 | tf_op jit(solution)/shard_map/dot_general | solution.py:171
  22.2 0.0 all-gather.4.cloned.1.call-update
  22.2 0.0 copy-start.9
  22.2 0.0 reduce-scatter.2.cloned.1.call-start
  22.2 0.0 copy-start.5
  22.2 0.0 copy-start.11
  22.3 6.1 %convolution_convert_fusion.2.x_ref = bf16[512,512]{1,0:T(8,128)(2,1)S(1)} fusion(bf16[4096,512]{1,0:T(8,128)(2,1)} %param.14, bf16[512,4096]{1,0:T(8,128)(2,1)} %param.12, f32[4096]{0:T(1024)S(1)} %copy-done.12, f32[512]{0:T(512)S(1)} %add_rsqrt_fusion), kind=kOutput, calls=%fused_computation.10 | convolution fusion | flops 2156134400 | bytes 8931328 | tf_op jit(solution)/shard_map/dot_general | solution.py:177
  28.4 0.0 copy-start.8
  28.4 5.3 %collective-permute-start = (bf16[16,512]{1,0:T(8,128)(2,1)S(1)}, bf16[16,512]{1,0:T(8,128)(2,1)S(1)}, u32[]{:S(2)}, u32[]{:S(2)}) collective-permute-start(bf16[16,512]{1,0:T(8,128)(2,1)S(1)} %slice.12), channel_id=1, source_target_pairs={{0,4},{4,8},{8,12},{12,16},{16,20},{20,24},{24,28},{1,5},{5,9},{9,... | collective-permute-start | bytes 49160 | tf_op jit(solution)/shard_map/ppermute | solution.py:179
  33.7 0.0 copy-done.9
  33.7 0.0 copy-done.5
  33.7 0.0 copy-done.11
  33.8 2.4 fusion.3.q_ref
  36.2 0.0 copy-done.8
  36.2 0.7 fusion.7.mix_ref
  36.9 0.0 collective-permute-done.rim_ref
  36.9 0.0 copy-start.10
  36.9 0.6 copy-done.10
  37.5 2.9 %pooling.1 = bf16[512,512]{1,0:T(8,128)(2,1)} custom-call(bf16[512,512]{1,0:T(8,128)(2,1)} %copy-done.8, bf16[16,512]{1,0:T(8,128)(2,1)} %copy-done.10, bf16[4,128,128]{2,1,0:T(8,128)(2,1)} %fusion.7.mix_ref, f32[1,512]{1,0:T(1,128)} %bitcast.25), custom_call_target="tpu_custom_call" | custom-call | flops 67108864 | bytes 1048576 | tf_op jit(solution)/shard_map/pooling/pallas_call | solution.py:63
  40.4 0.0 copy-start.1
  40.4 0.0 copy-start.2
  40.4 52.5 %all-gather.6.cloned.1.call-done = bf16[4096,512]{0,1:T(8,128)(2,1)} async-done(((bf16[512,512]{0,1:T(8,128)(2,1)}), bf16[4096,512]{0,1:T(8,128)(2,1)}) %all-gather.6.cloned.1.call-update) | async-done | bytes 4194320 | tf_op jit(solution)/shard_map/all_gather | solution.py:176
  93.0 6.5 %copy.16 = bf16[4096,512]{1,0:T(8,128)(2,1)} copy(bf16[4096,512]{0,1:T(8,128)(2,1)} %all-gather.6.cloned.1.call-done) | data formatting | bytes 8388608 | tf_op jit(solution)/shard_map/all_gather | solution.py:176
  99.4 66.7 %all-gather.4.cloned.1.call-done.k_ref = bf16[4096,512]{1,0:T(8,128)(2,1)} async-done(((bf16[512,512]{1,0:T(8,128)(2,1)}), bf16[4096,512]{1,0:T(8,128)(2,1)}) %all-gather.4.cloned.1.call-update) | async-done | bytes 4194320 | tf_op jit(solution)/shard_map/all_gather | solution.py:172
  166.1 0.0 copy-done.1
  166.1 0.0 copy-done.2
  166.1 0.0 copy-start
  166.1 2.2 copy-done
  168.3 0.0 copy-start.3
  168.3 9.6 %attend.1 = bf16[512,512]{1,0:T(8,128)(2,1)S(1)} custom-call(f32[4]{0:T(128)S(1)} %copy-done.1, bf16[512,512]{1,0:T(8,128)(2,1)S(1)} %fusion.3.q_ref, bf16[4096,512]{1,0:T(8,128)(2,1)S(1)} %copy-done, bf16[8,512,512]{2,1,0:T(8,128)(2,1)} %bitcast.23, f32[1,128]{1,0:T(1,128)S(1)} %bitcast.22), custom_call_target="tpu_custom_call" | custom-call | flops 8589934592 | bytes 8388608 | tf_op jit(solution)/shard_map/attend/pallas_call | solution.py:129
  177.9 0.0 copy-done.3
  177.9 0.0 copy-start.6
  177.9 0.0 copy-start.7
  177.9 2.3 fusion.12
  180.3 0.0 copy-done.6
  180.3 0.0 copy-done.7
  180.3 4.3 %add_convert_fusion = bf16[512,4096]{1,0:T(8,128)(2,1)} fusion(f32[512,4096]{1,0:T(8,128)S(1)} %fusion.12, bf16[512,512]{1,0:T(8,128)(2,1)S(1)} %copy-done.7, bf16[512,4096]{1,0:T(8,128)(2,1)S(1)} %copy-done.6), kind=kOutput, calls=%fused_computation.5 | convolution fusion | flops 2151677952 | bytes 17301504 | tf_op jit(solution)/shard_map/dot_general | solution.py:187
  184.6 0.0 reduce-scatter.2.cloned.1.call-update
  184.6 89.8 %reduce-scatter.2.cloned.1.call-done = bf16[128,4096]{1,0:T(8,128)(2,1)} async-done(((bf16[512,4096]{1,0:T(8,128)(2,1)}), bf16[128,4096]{1,0:T(8,128)(2,1)}) %reduce-scatter.2.cloned.1.call-update) | async-done | bytes 1048592 | tf_op jit(solution)/shard_map/reduce_scatter | solution.py:188
  (3 shorter events, 0.0 us)
Async XLA Ops:
  6.5 86.4 %all-gather.6.cloned.1.call-start = ((), (), s32[]{:S(2)}) async-start(), calls=%async_computation.3 | async-start | bytes 4718592 | tf_op jit(solution)/shard_map/all_gather | solution.py:176
  6.5 3.4 %copy-start.4 = (bf16[512,4096]{1,0:T(8,128)(2,1)S(1)}, bf16[512,4096]{1,0:T(8,128)(2,1)}, u32[]{:S(2)}) copy-start(bf16[512,4096]{1,0:T(8,128)(2,1)} %param.12) | copy-start | bytes 12582916
  10.0 5.5 %copy-start.12 = (f32[4096]{0:T(1024)S(1)}, f32[4096]{0:T(1024)}, u32[]{:S(2)}) copy-start(f32[4096]{0:T(1024)} %param.13) | copy-start | bytes 49156
  15.4 150.6 %all-gather.4.cloned.1.call-start = ((), (), s32[]{:S(2)}) async-start(), calls=%async_computation.1 | async-start | bytes 4718592 | tf_op jit(solution)/shard_map/all_gather | solution.py:172
  22.2 11.5 %copy-start.9 = (bf16[8,64,64]{2,1,0:T(8,128)(2,1)S(1)}, bf16[8,64,64]{2,1,0:T(8,128)(2,1)}, u32[]{:S(2)}) copy-start(bf16[8,64,64]{2,1,0:T(8,128)(2,1)} %param.18) | copy-start | bytes 196612
  22.2 252.3 %reduce-scatter.2.cloned.1.call-start = ((), (), s32[]{:S(2)}) async-start(), calls=%async_computation.2 | async-start | bytes 5242880 | tf_op jit(solution)/shard_map/reduce_scatter | solution.py:188
  22.2 11.5 %copy-start.5 = (bf16[512,4096]{1,0:T(8,128)(2,1)S(1)}, bf16[512,4096]{1,0:T(8,128)(2,1)}, u32[]{:S(2)}) copy-start(bf16[512,4096]{1,0:T(8,128)(2,1)} %param.12) | copy-start | bytes 12582916
  22.2 11.5 %copy-start.11 = (bf16[4096,512]{1,0:T(8,128)(2,1)S(1)}, bf16[4096,512]{1,0:T(8,128)(2,1)}, u32[]{:S(2)}) copy-start(bf16[4096,512]{1,0:T(8,128)(2,1)} %param.15) | copy-start | bytes 12582916
  28.4 7.8 %copy-start.8 = (bf16[512,512]{1,0:T(8,128)(2,1)}, bf16[512,512]{1,0:T(8,128)(2,1)S(1)}, u32[]{:S(2)}) copy-start(bf16[512,512]{1,0:T(8,128)(2,1)S(1)} %convolution_convert_fusion.2.x_ref) | copy-start | bytes 1572868
  28.4 8.5 %collective-permute-start = (bf16[16,512]{1,0:T(8,128)(2,1)S(1)}, bf16[16,512]{1,0:T(8,128)(2,1)S(1)}, u32[]{:S(2)}, u32[]{:S(2)}) collective-permute-start(bf16[16,512]{1,0:T(8,128)(2,1)S(1)} %slice.12), channel_id=1, source_target_pairs={{0,4},{4,8},{8,12},{12,16},{16,20},{20,24},{24,28},{1,5},{5,9},{9,... | collective-permute-start | bytes 49160 | tf_op jit(solution)/shard_map/ppermute | solution.py:179
  36.9 0.6 copy-start.10
  40.4 125.7 %copy-start.1 = (f32[4]{0:T(128)S(1)}, f32[4]{0:T(128)}, u32[]{:S(2)}) copy-start(f32[4]{0:T(128)} %lam_ref.1) | copy-start | bytes 52
  40.4 125.7 %copy-start.2 = (f32[128]{0:T(128)S(1)}, f32[128]{0:T(128)}, u32[]{:S(2)}) copy-start(f32[128]{0:T(128)} %param.21) | copy-start | bytes 1540
  166.1 2.2 copy-start
  168.3 9.6 %copy-start.3 = (bf16[512,4096]{1,0:T(8,128)(2,1)S(1)}, bf16[512,4096]{1,0:T(8,128)(2,1)}, u32[]{:S(2)}) copy-start(bf16[512,4096]{1,0:T(8,128)(2,1)} %param.23) | copy-start | bytes 12582916
  177.9 2.4 copy-start.6
  177.9 2.4 copy-start.7
Sparse Core Ops, SparseCore 0:
  15.6 77.3 all-gather.5
  95.1 70.9 all-gather.3
  184.8 89.6 reduce-scatter.1

commit v2 on v1

--- a/solution.py
+++ b/solution.py
@@ -70,28 +70,39 @@
     )(pool_in, rim, mix, pool_scale.reshape(1, width))
 
 
-def attend_kernel(lam_ref, q_ref, k_ref, v_ref, gain_ref, out_ref, stacked, peak, total, acc):
-    rows = q_ref.shape[0]
-    head = pl.program_id(0)
+def attend_kernel(lam_ref, all_ref, gain_ref, out_ref, turned, stacked, peak, total, acc):
+    parts = all_ref.shape[0]
+    sub = out_ref.shape[1]
+    rows = (all_ref.shape[1] - sub) // 2
+    chunk = min(CHUNK, 2 * sub)
+    step = pl.program_id(0)
+    share = rows // sub
     mine = lax.axis_index("sp")
-    query = q_ref[...]
+    head, place = mine // share, mine % share
+
+    @pl.when(step == 0)
+    def _():
+        @pl.loop(0, parts)
+        def _(index):
+            turned[index] = all_ref[index, rows : 2 * rows, :].T
+
+    query = all_ref[step, 2 * rows :, :]
     lane = lax.broadcasted_iota(jnp.int32, query.shape, 1)
-    stacked[:rows] = jnp.where(lane < HEAD, query, 0)
-    stacked[rows:] = jnp.where(lane < HEAD, 0, query)
+    stacked[:sub] = jnp.where(lane < HEAD, query, 0)
+    stacked[sub:] = jnp.where(lane < HEAD, 0, query)
 
     def block(index, first):
-        k = k_ref[pl.ds(pl.multiple_of(index * rows, rows), rows), :]
-        v = v_ref[index]
-        for start in range(0, 2 * rows, CHUNK):
-            cols = slice(start, start + CHUNK)
+        k = all_ref[index, :rows, :]
+        v = turned[index]
+        for start in range(0, 2 * sub, chunk):
+            cols = slice(start, start + chunk)
             scores = lax.dot_general(
                 k, stacked[cols], (((1,), (1,)), ((), ())), preferred_element_type=jnp.float32
             )
             if first:
                 key_seg = lax.broadcasted_iota(jnp.int32, (rows, 1), 0) // SEGMENT
-                query_seg = (
-                    start % rows + lax.broadcasted_iota(jnp.int32, (1, CHUNK), 1)
-                ) // SEGMENT
+                query_at = (start + lax.broadcasted_iota(jnp.int32, (1, chunk), 1)) % sub
+                query_seg = (place * sub + query_at) // SEGMENT
                 scores = jnp.where(key_seg <= query_seg, scores, neg_big)
                 top = jnp.max(scores, axis=0, keepdims=True)
             else:
@@ -109,47 +120,79 @@
                 total[:, cols] = total[:, cols] * shrink + summed
                 acc[:, cols] = acc[:, cols] * shrink + weighted
 
-    block(mine, True)
-
-    @pl.loop(0, mine)
+    block(step, True)
+
+    @pl.loop(0, step)
     def _(index):
         block(index, False)
 
     averaged = acc[...] / total[...]
-    blend = averaged[:, :rows] - lam_ref[head] * averaged[:, rows:]
+    blend = averaged[:, :sub] - lam_ref[head] * averaged[:, sub:]
     scaled = blend * lax.rsqrt(jnp.mean(blend * blend, axis=0, keepdims=True) + eps_norm)
-    out_ref[...] = (scaled.T * gain_ref[...] * out_scale).astype(jnp.bfloat16)
+    out_ref[0] = (scaled.T * gain_ref[...] * out_scale).astype(jnp.bfloat16)
 
 
 def attend(query, keys, values, lam, head_gain):
     rows, width = query.shape
     heads = width // VDIM
-    parts, tokens = values.shape[0], keys.shape[0]
-    work = rows * tokens * heads
-    return pl.pallas_call(
+    parts = lax.axis_size("sp")
+    share = parts // heads
+    sub = rows // share
+
+    def to_all(array):
+        by_head = array.reshape(rows, heads, VDIM).transpose(1, 0, 2)
+        return jnp.broadcast_to(by_head[:, None], (heads, share, rows, VDIM))
+
+    query = query.reshape(share, sub, heads, VDIM).transpose(2, 0, 1, 3)
+    sent = jnp.concatenate([to_all(keys), to_all(values), query], 2)
+    sent = sent.reshape(parts, 2 * rows + sub, VDIM)
+    received = lax.all_to_all(sent, "sp", 0, 0, tiled=True)
+    work = rows * rows * parts * parts // share
+    out = pl.pallas_call(
         attend_kernel,
-        grid=(heads,),
+        grid=(parts,),
         in_specs=[
             pl.BlockSpec(memory_space=pltpu.SMEM),
-            pl.BlockSpec((rows, VDIM), lambda h: (0, h)),
-            pl.BlockSpec((tokens, VDIM), lambda h: (0, h)),
-            pl.BlockSpec((parts, VDIM, rows), lambda h: (0, h, 0)),
-            pl.BlockSpec((1, VDIM), lambda h: (0, 0)),
+            pl.BlockSpec(received.shape, lambda i: (0, 0, 0)),
+            pl.BlockSpec((1, VDIM), lambda i: (0, 0)),
         ],
-        out_specs=pl.BlockSpec((rows, VDIM), lambda h: (0, h)),
-        out_shape=jax.ShapeDtypeStruct((rows, width), jnp.bfloat16),
+        out_specs=pl.BlockSpec((1, sub, VDIM), lambda i: (i, 0, 0)),
+        out_shape=jax.ShapeDtypeStruct((parts, sub, VDIM), jnp.bfloat16),
         scratch_shapes=[
-            pltpu.VMEM((2 * rows, VDIM), jnp.bfloat16),
-            pltpu.VMEM((1, 2 * rows), jnp.float32),
-            pltpu.VMEM((1, 2 * rows), jnp.float32),
-            pltpu.VMEM((VDIM, 2 * rows), jnp.float32),
+            pltpu.VMEM((parts, VDIM, rows), jnp.bfloat16),
+            pltpu.VMEM((2 * sub, VDIM), jnp.bfloat16),
+            pltpu.VMEM((1, 2 * sub), jnp.float32),
+            pltpu.VMEM((1, 2 * sub), jnp.float32),
+            pltpu.VMEM((VDIM, 2 * sub), jnp.float32),
         ],
         cost_estimate=pl.CostEstimate(
-            flops=work * 1024, bytes_accessed=4 * tokens * width, transcendentals=2 * work
+            flops=work * 512, bytes_accessed=2 * received.size, transcendentals=work
         ),
-        compiler_params=pltpu.CompilerParams(vmem_limit_bytes=48 * 2**20),
+        compiler_params=pltpu.CompilerParams(vmem_limit_bytes=40 * 2**20),
         name="attend",
-    )(lam, query, keys, values, head_gain.reshape(1, VDIM))
+    )(lam, received, head_gain.reshape(1, VDIM))
+    back = lax.all_to_all(out, "sp", 0, 0, tiled=True)
+    back = back.reshape(heads, share, sub, VDIM).transpose(1, 2, 0, 3)
+    return back.reshape(rows, width)
+
+
+def scatter_sum(term):
+    devices = lax.axis_size("tp")
+    pairs = [[i, i + 1] for i in range(0, devices, 2)]
+    across = [list(range(core, devices, 2)) for core in range(2)]
+    half = lax.psum_scatter(
+        term, "tp", scatter_dimension=0, axis_index_groups=pairs, tiled=True
+    )
+    return lax.psum_scatter(
+        half, "tp", scatter_dimension=0, axis_index_groups=across, tiled=True
+    )
+
+
+def by_core(array):
+    devices = lax.axis_size("tp")
+    rows, width = array.shape
+    split = array.reshape(devices // 2, 2, rows // devices, width)
+    return split.transpose(1, 0, 2, 3).reshape(rows, width)
 
 
 def body(
@@ -169,11 +212,7 @@
     count_rows = tokens.shape[0]
     normed = normalize(tokens, norm_gain)
     keys = jnp.dot(normed, w_key, preferred_element_type=jnp.float32).astype(jnp.bfloat16)
-    all_keys = lax.all_gather(keys, "sp", axis=0, tiled=True)
-    values = lax.dot_general(
-        w_value, normed, (((0,), (1,)), ((), ())), preferred_element_type=jnp.float32
-    ).astype(jnp.bfloat16)
-    all_values = lax.all_gather(values, "sp", axis=0, tiled=False)
+    values = jnp.dot(normed, w_value, preferred_element_type=jnp.float32).astype(jnp.bfloat16)
     pool_in = jnp.dot(normed, w_pool_in, preferred_element_type=jnp.float32).astype(jnp.bfloat16)
     devices = lax.axis_size("sp")
     rim = lax.ppermute(
@@ -183,16 +222,10 @@
         jnp.dot(normed, w_query, preferred_element_type=jnp.float32) * (HEAD ** (-0.5) * log2_e)
     ).astype(jnp.bfloat16)
     pool_out = pooling(pool_in, rim, pool_mix, pool_scale)
-    attn_out = attend(query, all_keys, all_values, lam, head_gain)
-    term = jnp.dot(pool_out, pool_proj, preferred_element_type=jnp.float32)
-    return lax.psum_scatter(
-        (term + jnp.dot(attn_out, attn_proj, preferred_element_type=jnp.float32)).astype(
-            jnp.bfloat16
-        ),
-        "tp",
-        scatter_dimension=0,
-        tiled=True,
-    )
+    attn_out = attend(query, keys, values, lam, head_gain)
+    term = jnp.dot(by_core(pool_out), pool_proj, preferred_element_type=jnp.float32)
+    term = term + jnp.dot(by_core(attn_out), attn_proj, preferred_element_type=jnp.float32)
+    return scatter_sum(term.astype(jnp.bfloat16))
 
 
 def solution(mesh):

time: 281 us -> 217 us (0.77)
  waiting for transfers between devices: 209 us -> 50.3 us
  blocking collectives: 0 us -> 66.5 us
  Pallas kernels: 12.5 us -> 39.4 us
  local copies, waits for them, and re-layouts: 9.53 us -> 3.61 us
  matrix products: 27.2 us -> 31.5 us
    all_gather x2 -> x0, waiting for transfers between devices: 119 us -> none  [the longest x1 66.7 us: body(): all_keys = lax.all_gather(keys, 'sp', axis=0, tiled=True)]
    all_to_all x0 -> x1, blocking collectives: none -> 66.5 us  [attend(): received = lax.all_to_all(sent, 'sp', 0, 0, tiled=True)]
    reduce_scatter x1 -> x2, waiting for transfers between devices: 89.8 us -> 49.6 us  [the longest x1 35.4 us: scatter_sum(): lax.psum_scatter(half, 'tp', scatter_dimension=0, axis_index_groups=acros...]
    pallas_call x1, Pallas kernels: 9.61 us -> 36.5 us  [attend(): pl.pallas_call(attend_kernel, grid=(parts,), in_specs=[pl.BlockSpec(memor...]
    all_gather x1 -> x0, local copies, waits for them, and re-layouts: 6.47 us -> none  [body(): all_values = lax.all_gather(values, 'sp', axis=0, tiled=False)]
    all_to_all x0 -> x1, starting transfers between devices: none -> 3.59 us  [attend(): back = lax.all_to_all(out, 'sp', 0, 0, tiled=True)]
    dot_general x1, matrix products: 2.4 us -> 5.85 us  [body(): jnp.dot(normed, w_query, preferred_element_type=jnp.float32)]
    dot_general x3, matrix products: 12.1 us -> 15 us  [the longest x1 5.94 us: body(): jnp.dot(normed, w_value, preferred_element_type=jnp.float32)]
  transfers between devices with their start and end apart: 4 -> 4, of which waited for: 3 -> 3; matrix products, arithmetic and copies ran while one was open for 8% -> 4% of each run, Pallas kernels for 1% -> 1%
where the time goes in v2:
time: 217 us
  blocking collectives  66.5 us (31%)
  waiting for transfers between devices  50.3 us (23%)
  Pallas kernels  39.4 us (18%)
  matrix products  31.5 us (15%)
  between operations  13.6 us (6%)
  starting transfers between devices  7.59 us (3%)
  other arithmetic  4.16 us (2%)
  local copies, waits for them, and re-layouts  3.61 us (2%)
    all_to_all x1, blocking collectives, attend(): received = lax.all_to_all(sent, 'sp', 0, 0, tiled=True)  66.5 us
    pallas_call x1, Pallas kernels, attend(): pl.pallas_call(attend_kernel, grid=(parts,), in_specs=[pl.BlockSpec(memor...  36.5 us
    reduce_scatter x1, waiting for transfers between devices, scatter_sum(): lax.psum_scatter(half, 'tp', scatter_dimension=0, axis_index_groups=acros...  35.4 us
    reduce_scatter x1, waiting for transfers between devices, scatter_sum(): lax.psum_scatter(term, 'tp', scatter_dimension=0, axis_index_groups=pairs...  14.1 us
    dot_general x1, matrix products, body(): jnp.dot(normed, w_value, preferred_element_type=jnp.float32)  5.94 us
    dot_general x1, matrix products, body(): jnp.dot(normed, w_query, preferred_element_type=jnp.float32)  5.85 us
    dot_general x1, matrix products, body(): jnp.dot(normed, w_pool_in, preferred_element_type=jnp.float32)  5.84 us
    dot_general x1, matrix products, body(): jnp.dot(normed, w_key, preferred_element_type=jnp.float32)  4.79 us
  transfers between devices with their start and end apart: 4, of which 3 were waited for; matrix products, arithmetic and copies ran while one was open for 4% of the time, Pallas kernels for 1%

profile of v2, /device:TPU:0, one launch (start us, length us, event | category | flops | bytes accessed | tf_op | source)
XLA Modules:
  0.0 216.6 jit_solution(10338262519384780112)
XLA Ops:
  6.5 0.0 copy-start.2
  6.5 3.2 %fusion = f32[512]{0:T(512)S(1)} fusion(bf16[512,4096]{1,0:T(8,128)(2,1)} %param.12), kind=kLoop, calls=%fused_computation.2 | loop fusion | flops 6290944 | bytes 4196352 | tf_op jit(solution)/shard_map/reduce_sum | solution.py:25
  9.8 0.2 copy-done.2
  10.0 0.0 copy-start.7
  10.0 4.8 %convolution_convert_fusion.1 = bf16[512,512]{0,1:T(8,128)(2,1)S(1)} fusion(bf16[4096,512]{1,0:T(8,128)(2,1)} %param.16, bf16[512,4096]{1,0:T(8,128)(2,1)S(1)} %copy-done.2, f32[4096]{0:T(1024)} %param.13, f32[512]{0:T(512)S(1)} %add_rsqrt_fusion), kind=kOutput, calls=%fused_computation.10 | convolution fusion | flops 2156134400 | bytes 8931328 | tf_op jit(solution)/shard_map/dot_general | solution.py:214
  14.8 0.3 copy.19
  15.1 0.0 copy-done.7
  15.1 5.9 %convolution_convert_fusion = bf16[512,512]{0,1:T(8,128)(2,1)S(1)} fusion(bf16[4096,512]{1,0:T(8,128)(2,1)} %param.17, bf16[512,4096]{1,0:T(8,128)(2,1)} %param.12, f32[4096]{0:T(1024)S(1)} %copy-done.7, f32[512]{0:T(512)S(1)} %add_rsqrt_fusion), kind=kOutput, calls=%fused_computation.9 | convolution fusion | flops 2156134400 | bytes 8931328 | tf_op jit(solution)/shard_map/dot_general | solution.py:215
  21.0 0.3 copy.20
  21.3 5.8 %fusion.3 = bf16[512,512]{1,0:T(8,128)(2,1)S(1)} fusion(bf16[4096,512]{1,0:T(8,128)(2,1)} %param.15, bf16[512,4096]{1,0:T(8,128)(2,1)} %param.12, f32[4096]{0:T(1024)S(1)} %copy-done.7, f32[512]{0:T(512)S(1)} %add_rsqrt_fusion), kind=kOutput, calls=%fused_computation.8 | convolution fusion | flops 2156396544 | bytes 8931328 | tf_op jit(solution)/shard_map/dot_general | solution.py:222
  27.2 0.1 reshape.50
  27.3 0.1 copy.29
  27.4 0.1 broadcast_in_dim.4
  27.5 0.1 broadcast_in_dim.5
  27.7 0.0 copy-start
  27.7 0.0 copy-start.1
  27.7 0.2 pad_maximum_fusion
  27.9 66.5 %all_to_all.10.all_ref = bf16[8,1280,128]{2,1,0:T(8,128)(2,1)S(1)} all-to-all(bf16[8,1280,128]{2,1,0:T(8,128)(2,1)S(1)} %bitcast.40), channel_id=1, replica_groups=mesh['sp'=8,'tp'=4] {'sp'}, dimensions={0} | all-to-all | bytes 5242880 | tf_op jit(solution)/shard_map/all_to_all | solution.py:149
  94.4 0.0 copy-done
  94.4 0.0 copy-done.1
  94.4 36.5 %attend.1 = bf16[8,256,128]{2,1,0:T(8,128)(2,1)} custom-call(f32[4]{0:T(128)S(1)} %copy-done, bf16[8,1280,128]{2,1,0:T(8,128)(2,1)S(1)} %all_to_all.10.all_ref, f32[1,128]{1,0:T(1,128)S(1)} %bitcast.39), custom_call_target="tpu_custom_call" | custom-call | flops 4294967296 | bytes 2621440 | tf_op jit(solution)/shard_map/attend/pallas_call | solution.py:151
  130.9 3.6 %all-to-all-start.1 = ((bf16[8,256,128]{2,1,0:T(8,128)(2,1)}), bf16[8,256,128]{2,1,0:T(8,128)(2,1)S(1)}, u32[]{:S(2)}, u32[]{:S(2)}) async-start(bf16[8,256,128]{2,1,0:T(8,128)(2,1)} %attend.1), calls=%async_computation.1 | async-start | bytes 1048576 | tf_op jit(solution)/shard_map/all_to_all | solution.py:174
  134.5 0.0 copy-start.5
  134.5 0.2 reduce-scatter.3.cloned.1.call-start
  134.8 5.8 %convolution_convert_fusion.2.x_ref = bf16[512,512]{1,0:T(8,128)(2,1)S(1)} fusion(bf16[4096,512]{1,0:T(8,128)(2,1)} %param.14, bf16[512,4096]{1,0:T(8,128)(2,1)} %param.12, f32[4096]{0:T(1024)S(1)} %copy-done.7, f32[512]{0:T(512)S(1)} %add_rsqrt_fusion), kind=kOutput, calls=%fused_computation.11 | convolution fusion | flops 2156134400 | bytes 8931328 | tf_op jit(solution)/shard_map/dot_general | solution.py:216
  140.6 0.0 copy-start.4
  140.6 3.7 %collective-permute-start = (bf16[16,512]{1,0:T(8,128)(2,1)S(1)}, bf16[16,512]{1,0:T(8,128)(2,1)S(1)}, u32[]{:S(2)}, u32[]{:S(2)}) collective-permute-start(bf16[16,512]{1,0:T(8,128)(2,1)S(1)} %slice.12), channel_id=1, source_target_pairs={{0,4},{4,8},{8,12},{12,16},{16,20},{20,24},{24,28},{1,5},{5,9},{9,... | collective-permute-start | bytes 49160 | tf_op jit(solution)/shard_map/ppermute | solution.py:218
  144.4 0.0 copy-done.5
  144.4 0.8 fusion.6.mix_ref
  145.2 0.6 collective-permute-done.rim_ref
  145.8 0.0 copy-start.6
  145.8 0.0 copy-done.4
  145.8 0.6 copy-done.6
  146.4 2.8 %pooling.1 = bf16[512,512]{1,0:T(8,128)(2,1)} custom-call(bf16[512,512]{1,0:T(8,128)(2,1)} %copy-done.4, bf16[16,512]{1,0:T(8,128)(2,1)} %copy-done.6, bf16[4,128,128]{2,1,0:T(8,128)(2,1)} %fusion.6.mix_ref, f32[1,512]{1,0:T(1,128)} %bitcast.51), custom_call_target="tpu_custom_call" | custom-call | flops 67108864 | bytes 1048576 | tf_op jit(solution)/shard_map/pooling/pallas_call | solution.py:63
  149.3 1.1 copy.18
  150.3 0.0 all-to-all-done.1
  150.3 0.4 copy.28
  150.8 0.2 reshape_reshape.3
  151.0 0.0 copy-start.3
  151.0 4.8 %fusion.11 = f32[512,4096]{1,0:T(8,128)S(1)} fusion(bf16[512,512]{1,0:T(8,128)(2,1)S(1)} %bitcast.43, bf16[512,4096]{1,0:T(8,128)(2,1)} %param.23), kind=kOutput, calls=%fused_computation.22 | convolution fusion | flops 2147483648 | bytes 13107200 | tf_op jit(solution)/shard_map/dot_general | solution.py:227
  155.8 0.0 copy-done.3
  155.8 4.3 %add_convert_fusion = bf16[512,4096]{1,0:T(8,128)(2,1)} fusion(f32[512,4096]{1,0:T(8,128)S(1)} %fusion.11, bf16[512,512]{1,0:T(8,128)(2,1)S(1)} %bitcast.41, bf16[512,4096]{1,0:T(8,128)(2,1)S(1)} %copy-done.3), kind=kOutput, calls=%fused_computation.5 | convolution fusion | flops 2151677952 | bytes 17301504 | tf_op jit(solution)/shard_map/dot_general | solution.py:226
  160.1 0.0 reduce-scatter.3.cloned.1.call-update
  160.1 0.0 reduce-scatter.5.cloned.1.call-start
  160.2 14.1 %reduce-scatter.3.cloned.1.call-done = bf16[256,4096]{1,0:T(8,128)(2,1)} async-done(((bf16[512,4096]{1,0:T(8,128)(2,1)}), bf16[256,4096]{1,0:T(8,128)(2,1)}) %reduce-scatter.3.cloned.1.call-update) | async-done | bytes 2097168 | tf_op jit(solution)/shard_map/reduce_scatter | solution.py:183
  174.3 0.0 reduce-scatter.5.cloned.1.call-update
  174.3 35.4 %reduce-scatter.5.cloned.1.call-done = bf16[128,4096]{1,0:T(8,128)(2,1)} async-done(((bf16[256,4096]{1,0:T(8,128)(2,1)}), bf16[128,4096]{1,0:T(8,128)(2,1)}) %reduce-scatter.5.cloned.1.call-update) | async-done | bytes 1048592 | tf_op jit(solution)/shard_map/reduce_scatter | solution.py:186
  (4 shorter events, 0.1 us)
Async XLA Ops:
  6.5 3.4 %copy-start.2 = (bf16[512,4096]{1,0:T(8,128)(2,1)S(1)}, bf16[512,4096]{1,0:T(8,128)(2,1)}, u32[]{:S(2)}) copy-start(bf16[512,4096]{1,0:T(8,128)(2,1)} %param.12) | copy-start | bytes 12582916
  10.0 5.1 %copy-start.7 = (f32[4096]{0:T(1024)S(1)}, f32[4096]{0:T(1024)}, u32[]{:S(2)}) copy-start(f32[4096]{0:T(1024)} %param.13) | copy-start | bytes 49156
  27.7 66.8 %copy-start = (f32[4]{0:T(128)S(1)}, f32[4]{0:T(128)}, u32[]{:S(2)}) copy-start(f32[4]{0:T(128)} %lam_ref.1) | copy-start | bytes 52
  27.7 66.7 %copy-start.1 = (f32[128]{0:T(128)S(1)}, f32[128]{0:T(128)}, u32[]{:S(2)}) copy-start(f32[128]{0:T(128)} %param.21) | copy-start | bytes 1540
  130.9 19.4 %all-to-all-start.1 = ((bf16[8,256,128]{2,1,0:T(8,128)(2,1)}), bf16[8,256,128]{2,1,0:T(8,128)(2,1)S(1)}, u32[]{:S(2)}, u32[]{:S(2)}) async-start(bf16[8,256,128]{2,1,0:T(8,128)(2,1)} %attend.1), calls=%async_computation.1 | async-start | bytes 1048576 | tf_op jit(solution)/shard_map/all_to_all | solution.py:174
  134.5 9.8 %copy-start.5 = (bf16[8,64,64]{2,1,0:T(8,128)(2,1)S(1)}, bf16[8,64,64]{2,1,0:T(8,128)(2,1)}, u32[]{:S(2)}) copy-start(bf16[8,64,64]{2,1,0:T(8,128)(2,1)} %param.18) | copy-start | bytes 196612
  134.5 39.8 %reduce-scatter.3.cloned.1.call-start = ((), (), s32[]{:S(2)}) async-start(), calls=%async_computation.4 | async-start | bytes 6291456 | tf_op jit(solution)/shard_map/reduce_scatter | solution.py:183
  140.6 5.2 %copy-start.4 = (bf16[512,512]{1,0:T(8,128)(2,1)}, bf16[512,512]{1,0:T(8,128)(2,1)S(1)}, u32[]{:S(2)}) copy-start(bf16[512,512]{1,0:T(8,128)(2,1)S(1)} %convolution_convert_fusion.2.x_ref) | copy-start | bytes 1572868
  140.6 5.2 %collective-permute-start = (bf16[16,512]{1,0:T(8,128)(2,1)S(1)}, bf16[16,512]{1,0:T(8,128)(2,1)S(1)}, u32[]{:S(2)}, u32[]{:S(2)}) collective-permute-start(bf16[16,512]{1,0:T(8,128)(2,1)S(1)} %slice.12), channel_id=1, source_target_pairs={{0,4},{4,8},{8,12},{12,16},{16,20},{20,24},{24,28},{1,5},{5,9},{9,... | collective-permute-start | bytes 49160 | tf_op jit(solution)/shard_map/ppermute | solution.py:218
  145.8 0.6 copy-start.6
  151.0 4.8 %copy-start.3 = (bf16[512,4096]{1,0:T(8,128)(2,1)S(1)}, bf16[512,4096]{1,0:T(8,128)(2,1)}, u32[]{:S(2)}) copy-start(bf16[512,4096]{1,0:T(8,128)(2,1)} %param.22) | copy-start | bytes 12582916
  160.1 49.7 %reduce-scatter.5.cloned.1.call-start = ((), (), s32[]{:S(2)}) async-start(), calls=%async_computation.5 | async-start | bytes 3145728 | tf_op jit(solution)/shard_map/reduce_scatter | solution.py:186
Sparse Core Ops, SparseCore 0:
  160.2 14.0 reduce-scatter.2
  176.6 33.1 reduce-scatter.4

commit v3 on v2

--- a/solution.py
+++ b/solution.py
@@ -70,10 +70,9 @@
     )(pool_in, rim, mix, pool_scale.reshape(1, width))
 
 
-def attend_kernel(lam_ref, all_ref, gain_ref, out_ref, turned, stacked, peak, total, acc):
-    parts = all_ref.shape[0]
+def attend_kernel(lam_ref, k_ref, v_ref, q_ref, gain_ref, out_ref, turned, stacked, peak, total, acc):
+    parts, rows = k_ref.shape[:2]
     sub = out_ref.shape[1]
-    rows = (all_ref.shape[1] - sub) // 2
     chunk = min(CHUNK, 2 * sub)
     step = pl.program_id(0)
     share = rows // sub
@@ -84,15 +83,15 @@
     def _():
         @pl.loop(0, parts)
         def _(index):
-            turned[index] = all_ref[index, rows : 2 * rows, :].T
-
-    query = all_ref[step, 2 * rows :, :]
+            turned[index] = v_ref[index].T
+
+    query = q_ref[step]
     lane = lax.broadcasted_iota(jnp.int32, query.shape, 1)
     stacked[:sub] = jnp.where(lane < HEAD, query, 0)
     stacked[sub:] = jnp.where(lane < HEAD, 0, query)
 
     def block(index, first):
-        k = all_ref[index, :rows, :]
+        k = k_ref[index]
         v = turned[index]
         for start in range(0, 2 * sub, chunk):
             cols = slice(start, start + chunk)
@@ -141,19 +140,24 @@
 
     def to_all(array):
         by_head = array.reshape(rows, heads, VDIM).transpose(1, 0, 2)
-        return jnp.broadcast_to(by_head[:, None], (heads, share, rows, VDIM))
+        copies = jnp.broadcast_to(by_head[:, None], (heads, share, rows, VDIM))
+        copies = copies.reshape(parts, rows, VDIM)
+        return lax.all_to_all(copies, "sp", 0, 0, tiled=True)
 
     query = query.reshape(share, sub, heads, VDIM).transpose(2, 0, 1, 3)
-    sent = jnp.concatenate([to_all(keys), to_all(values), query], 2)
-    sent = sent.reshape(parts, 2 * rows + sub, VDIM)
-    received = lax.all_to_all(sent, "sp", 0, 0, tiled=True)
+    query = query.reshape(parts, sub, VDIM)
+    received = (
+        to_all(keys),
+        to_all(values),
+        lax.all_to_all(query, "sp", 0, 0, tiled=True),
+    )
     work = rows * rows * parts * parts // share
     out = pl.pallas_call(
         attend_kernel,
         grid=(parts,),
         in_specs=[
             pl.BlockSpec(memory_space=pltpu.SMEM),
-            pl.BlockSpec(received.shape, lambda i: (0, 0, 0)),
+            *[pl.BlockSpec(array.shape, lambda i: (0, 0, 0)) for array in received],
             pl.BlockSpec((1, VDIM), lambda i: (0, 0)),
         ],
         out_specs=pl.BlockSpec((1, sub, VDIM), lambda i: (i, 0, 0)),
@@ -166,33 +170,14 @@
             pltpu.VMEM((VDIM, 2 * sub), jnp.float32),
         ],
         cost_estimate=pl.CostEstimate(
-            flops=work * 512, bytes_accessed=2 * received.size, transcendentals=work
+            flops=work * 512, bytes_accessed=6 * received[0].size, transcendentals=work
         ),
         compiler_params=pltpu.CompilerParams(vmem_limit_bytes=40 * 2**20),
         name="attend",
-    )(lam, received, head_gain.reshape(1, VDIM))
+    )(lam, *received, head_gain.reshape(1, VDIM))
     back = lax.all_to_all(out, "sp", 0, 0, tiled=True)
     back = back.reshape(heads, share, sub, VDIM).transpose(1, 2, 0, 3)
     return back.reshape(rows, width)
-
-
-def scatter_sum(term):
-    devices = lax.axis_size("tp")
-    pairs = [[i, i + 1] for i in range(0, devices, 2)]
-    across = [list(range(core, devices, 2)) for core in range(2)]
-    half = lax.psum_scatter(
-        term, "tp", scatter_dimension=0, axis_index_groups=pairs, tiled=True
-    )
-    return lax.psum_scatter(
-        half, "tp", scatter_dimension=0, axis_index_groups=across, tiled=True
-    )
-
-
-def by_core(array):
-    devices = lax.axis_size("tp")
-    rows, width = array.shape
-    split = array.reshape(devices // 2, 2, rows // devices, width)
-    return split.transpose(1, 0, 2, 3).reshape(rows, width)
 
 
 def body(
@@ -223,9 +208,11 @@
     ).astype(jnp.bfloat16)
     pool_out = pooling(pool_in, rim, pool_mix, pool_scale)
     attn_out = attend(query, keys, values, lam, head_gain)
-    term = jnp.dot(by_core(pool_out), pool_proj, preferred_element_type=jnp.float32)
-    term = term + jnp.dot(by_core(attn_out), attn_proj, preferred_element_type=jnp.float32)
-    return scatter_sum(term.astype(jnp.bfloat16))
+    term = jnp.dot(pool_out, pool_proj, preferred_element_type=jnp.float32)
+    term = term + jnp.dot(attn_out, attn_proj, preferred_element_type=jnp.float32)
+    return lax.psum_scatter(
+        term.astype(jnp.bfloat16), "tp", scatter_dimension=0, tiled=True
+    )
 
 
 def solution(mesh):

time: 217 us -> 216 us (level)
  blocking collectives: 66.5 us -> 29.3 us
  waiting for transfers between devices: 50.3 us -> 75.4 us
  starting transfers between devices: 7.59 us -> 18.5 us
    all_to_all x1, blocking collectives: 66.5 us -> 29.3 us  [to_all(): return lax.all_to_all(copies, 'sp', 0, 0, tiled=True)]
    all_to_all x0 -> x2, waiting for transfers between devices: none -> 28 us  [the longest x1 19.7 us: to_all(): return lax.all_to_all(copies, 'sp', 0, 0, tiled=True)]
    all_to_all x0 -> x2, starting transfers between devices: none -> 10.9 us  [the longest x1 7.28 us: attend(): lax.all_to_all(query, 'sp', 0, 0, tiled=True)]
    reduce_scatter x2 -> x1, waiting for transfers between devices: 49.6 us -> 46.7 us  [body(): lax.psum_scatter(term.astype(jnp.bfloat16), 'tp', scatter_dimension=0, ti...]
  transfers between devices with their start and end apart: 4 -> 5, of which waited for: 3 -> 4; matrix products, arithmetic and copies ran while one was open for 4% -> 9% of each run, Pallas kernels for 1% -> 1%
where the time goes in v3:
time: 216 us
  waiting for transfers between devices  75.4 us (35%)
  Pallas kernels  39.6 us (18%)
  matrix products  31.3 us (14%)
  blocking collectives  29.3 us (14%)
  starting transfers between devices  18.5 us (9%)
  between operations  13.6 us (6%)
  local copies, waits for them, and re-layouts  4.05 us (2%)
  other arithmetic  3.98 us (2%)
    reduce_scatter x1, waiting for transfers between devices, body(): lax.psum_scatter(term.astype(jnp.bfloat16), 'tp', scatter_dimension=0, ti...  46.7 us
    pallas_call x1, Pallas kernels, attend(): pl.pallas_call(attend_kernel, grid=(parts,), in_specs=[pl.BlockSpec(memor...  36.7 us
    all_to_all x1, blocking collectives, to_all(): return lax.all_to_all(copies, 'sp', 0, 0, tiled=True)  29.3 us
    all_to_all x1, waiting for transfers between devices, to_all(): return lax.all_to_all(copies, 'sp', 0, 0, tiled=True)  19.7 us
    all_to_all x1, waiting for transfers between devices, attend(): lax.all_to_all(query, 'sp', 0, 0, tiled=True)  8.26 us
    all_to_all x1, starting transfers between devices, attend(): lax.all_to_all(query, 'sp', 0, 0, tiled=True)  7.28 us
    dot_general x1, matrix products, body(): jnp.dot(normed, w_key, preferred_element_type=jnp.float32)  5.94 us
    dot_general x1, matrix products, body(): jnp.dot(normed, w_value, preferred_element_type=jnp.float32)  5.93 us
  transfers between devices with their start and end apart: 5, of which 4 were waited for; matrix products, arithmetic and copies ran while one was open for 9% of the time, Pallas kernels for 1%

profile of v3, /device:TPU:0, one launch (start us, length us, event | category | flops | bytes accessed | tf_op | source)
XLA Modules:
  0.0 215.7 jit_solution(15513896803798074668)
XLA Ops:
  6.5 0.0 copy-start.2
  6.5 3.2 %fusion = f32[512]{0:T(512)S(1)} fusion(bf16[512,4096]{1,0:T(8,128)(2,1)} %param.12), kind=kLoop, calls=%fused_computation.2 | loop fusion | flops 6290944 | bytes 4196352 | tf_op jit(solution)/shard_map/reduce_sum | solution.py:25
  9.8 0.2 copy-done.2
  10.0 0.0 copy-start.8
  10.0 4.6 %fusion.3 = bf16[512,512]{1,0:T(8,128)(2,1)S(1)} fusion(bf16[4096,512]{1,0:T(8,128)(2,1)} %param.15, bf16[512,4096]{1,0:T(8,128)(2,1)S(1)} %copy-done.2, f32[4096]{0:T(1024)} %param.13, f32[512]{0:T(512)S(1)} %add_rsqrt_fusion), kind=kOutput, calls=%fused_computation.7 | convolution fusion | flops 2156396544 | bytes 8931328 | tf_op jit(solution)/shard_map/dot_general | solution.py:207
  14.6 0.1 reshape.50
  14.7 0.9 copy.20
  15.6 7.3 %all-to-all-start.2 = ((bf16[8,256,128]{2,1,0:T(8,128)(2,1)}), bf16[8,256,128]{2,1,0:T(8,128)(2,1)S(1)}, u32[]{:S(2)}, u32[]{:S(2)}) async-start(bf16[8,256,128]{2,1,0:T(8,128)(2,1)} %bitcast.11), calls=%async_computation.2 | async-start | bytes 1048576 | tf_op jit(solution)/shard_map/all_to_all | solution.py:152
  22.9 0.0 copy-done.8
  22.9 5.9 %convolution_convert_fusion.1 = bf16[512,512]{0,1:T(8,128)(2,1)S(1)} fusion(bf16[4096,512]{1,0:T(8,128)(2,1)} %param.16, bf16[512,4096]{1,0:T(8,128)(2,1)} %param.12, f32[4096]{0:T(1024)S(1)} %copy-done.8, f32[512]{0:T(512)S(1)} %add_rsqrt_fusion), kind=kOutput, calls=%fused_computation.9 | convolution fusion | flops 2156134400 | bytes 8931328 | tf_op jit(solution)/shard_map/dot_general | solution.py:199
  28.9 0.3 copy.18
  29.1 8.3 %all-to-all-done.2.q_ref = bf16[8,256,128]{2,1,0:T(8,128)(2,1)S(1)} async-done(((bf16[8,256,128]{2,1,0:T(8,128)(2,1)}), bf16[8,256,128]{2,1,0:T(8,128)(2,1)S(1)}, u32[]{:S(2)}, u32[]{:S(2)}) %all-to-all-start.2) | async-done | bytes 524320 | tf_op jit(solution)/shard_map/all_to_all | solution.py:152
  37.4 1.1 broadcast_in_dim.4
  38.5 3.6 %all-to-all-start = ((bf16[8,512,128]{2,1,0:T(8,128)(2,1)}), bf16[8,512,128]{2,1,0:T(8,128)(2,1)S(1)}, u32[]{:S(2)}, u32[]{:S(2)}) async-start(bf16[8,512,128]{2,1,0:T(8,128)(2,1)} %bitcast.6), calls=%async_computation | async-start | bytes 2097152 | tf_op jit(solution)/shard_map/all_to_all | solution.py:145
  42.1 5.9 %convolution_convert_fusion = bf16[512,512]{0,1:T(8,128)(2,1)S(1)} fusion(bf16[4096,512]{1,0:T(8,128)(2,1)} %param.17, bf16[512,4096]{1,0:T(8,128)(2,1)} %param.12, f32[4096]{0:T(1024)S(1)} %copy-done.8, f32[512]{0:T(512)S(1)} %add_rsqrt_fusion), kind=kOutput, calls=%fused_computation.8 | convolution fusion | flops 2156134400 | bytes 8931328 | tf_op jit(solution)/shard_map/dot_general | solution.py:200
  48.1 0.0 copy-start
  48.1 0.0 copy-start.1
  48.1 0.3 copy.19
  48.4 19.7 %all-to-all-done.k_ref = bf16[8,512,128]{2,1,0:T(8,128)(2,1)S(1)} async-done(((bf16[8,512,128]{2,1,0:T(8,128)(2,1)}), bf16[8,512,128]{2,1,0:T(8,128)(2,1)S(1)}, u32[]{:S(2)}, u32[]{:S(2)}) %all-to-all-start) | async-done | bytes 1048608 | tf_op jit(solution)/shard_map/all_to_all | solution.py:145
  68.1 0.1 broadcast_in_dim.5
  68.2 29.3 %all_to_all.20.v_ref = bf16[8,512,128]{2,1,0:T(8,128)(2,1)S(1)} all-to-all(bf16[8,512,128]{2,1,0:T(8,128)(2,1)S(1)} %bitcast.37), channel_id=1, replica_groups=mesh['sp'=8,'tp'=4] {'sp'}, dimensions={0} | all-to-all | bytes 2097152 | tf_op jit(solution)/shard_map/all_to_all | solution.py:145
  97.6 0.0 copy-done
  97.6 0.0 copy-done.1
  97.6 36.7 %attend.1 = bf16[8,256,128]{2,1,0:T(8,128)(2,1)} custom-call(f32[4]{0:T(128)S(1)} %copy-done, bf16[8,512,128]{2,1,0:T(8,128)(2,1)S(1)} %all-to-all-done.k_ref, bf16[8,512,128]{2,1,0:T(8,128)(2,1)S(1)} %all_to_all.20.v_ref, bf16[8,256,128]{2,1,0:T(8,128)(2,1)S(1)} %all-to-all-done.2.q_ref, f32[1,128]{1,0:T(1,128)S(1)} %bitcast.36), custom_call_target="tpu_custom_call" | custom-call | flops 4294967296 | bytes 3145728 | tf_op jit(solution)/shard_map/attend/pallas_call | solution.py:155
  134.3 3.6 %all-to-all-start.3 = ((bf16[8,256,128]{2,1,0:T(8,128)(2,1)}), bf16[8,256,128]{2,1,0:T(8,128)(2,1)S(1)}, u32[]{:S(2)}, u32[]{:S(2)}) async-start(bf16[8,256,128]{2,1,0:T(8,128)(2,1)} %attend.1), calls=%async_computation.3 | async-start | bytes 1048576 | tf_op jit(solution)/shard_map/all_to_all | solution.py:178
  137.9 0.0 copy-start.6
  137.9 0.2 reduce-scatter.2.cloned.1.call-start
  138.2 5.8 %convolution_convert_fusion.2.x_ref = bf16[512,512]{1,0:T(8,128)(2,1)S(1)} fusion(bf16[4096,512]{1,0:T(8,128)(2,1)} %param.14, bf16[512,4096]{1,0:T(8,128)(2,1)} %param.12, f32[4096]{0:T(1024)S(1)} %copy-done.8, f32[512]{0:T(512)S(1)} %add_rsqrt_fusion), kind=kOutput, calls=%fused_computation.10 | convolution fusion | flops 2156134400 | bytes 8931328 | tf_op jit(solution)/shard_map/dot_general | solution.py:201
  144.0 0.0 copy-start.5
  144.0 3.7 %collective-permute-start = (bf16[16,512]{1,0:T(8,128)(2,1)S(1)}, bf16[16,512]{1,0:T(8,128)(2,1)S(1)}, u32[]{:S(2)}, u32[]{:S(2)}) collective-permute-start(bf16[16,512]{1,0:T(8,128)(2,1)S(1)} %slice.12), channel_id=1, source_target_pairs={{0,4},{4,8},{8,12},{12,16},{16,20},{20,24},{24,28},{1,5},{5,9},{9,... | collective-permute-start | bytes 49160 | tf_op jit(solution)/shard_map/ppermute | solution.py:203
  147.8 0.0 copy-done.6
  147.8 0.7 fusion.9.mix_ref
  148.5 0.7 collective-permute-done.rim_ref
  149.2 0.0 copy-start.7
  149.2 0.0 copy-done.5
  149.2 0.6 copy-done.7
  149.8 2.9 %pooling.1 = bf16[512,512]{1,0:T(8,128)(2,1)} custom-call(bf16[512,512]{1,0:T(8,128)(2,1)} %copy-done.5, bf16[16,512]{1,0:T(8,128)(2,1)} %copy-done.7, bf16[4,128,128]{2,1,0:T(8,128)(2,1)} %fusion.9.mix_ref, f32[1,512]{1,0:T(1,128)} %bitcast.43), custom_call_target="tpu_custom_call" | custom-call | flops 67108864 | bytes 1048576 | tf_op jit(solution)/shard_map/pooling/pallas_call | solution.py:63
  152.7 0.0 all-to-all-done.3
  152.7 0.4 copy.21
  153.1 0.0 copy-start.3
  153.1 0.0 copy-start.4
  153.1 4.7 %fusion.4 = f32[512,4096]{1,0:T(8,128)S(1)} fusion(bf16[512,4096]{1,0:T(8,128)(2,1)} %param.23, bf16[64,8,4,128]{3,2,1,0:T(4,128)(2,1)S(1)} %bitcast.38), kind=kOutput, calls=%fused_computation.11 | convolution fusion | flops 2147483648 | bytes 13107200 | tf_op jit(solution)/shard_map/dot_general | solution.py:212
  157.8 0.0 copy-done.3
  157.8 0.0 copy-done.4
  157.8 4.3 %add_convert_fusion = bf16[512,4096]{1,0:T(8,128)(2,1)} fusion(f32[512,4096]{1,0:T(8,128)S(1)} %fusion.4, bf16[512,512]{1,0:T(8,128)(2,1)S(1)} %copy-done.4, bf16[512,4096]{1,0:T(8,128)(2,1)S(1)} %copy-done.3), kind=kOutput, calls=%fused_computation.5 | convolution fusion | flops 2151677952 | bytes 17301504 | tf_op jit(solution)/shard_map/dot_general | solution.py:211
  162.1 0.0 reduce-scatter.2.cloned.1.call-update
  162.1 46.7 %reduce-scatter.2.cloned.1.call-done = bf16[128,4096]{1,0:T(8,128)(2,1)} async-done(((bf16[512,4096]{1,0:T(8,128)(2,1)}), bf16[128,4096]{1,0:T(8,128)(2,1)}) %reduce-scatter.2.cloned.1.call-update) | async-done | bytes 1048592 | tf_op jit(solution)/shard_map/reduce_scatter | solution.py:213
  (3 shorter events, 0.0 us)
Async XLA Ops:
  6.5 3.4 %copy-start.2 = (bf16[512,4096]{1,0:T(8,128)(2,1)S(1)}, bf16[512,4096]{1,0:T(8,128)(2,1)}, u32[]{:S(2)}) copy-start(bf16[512,4096]{1,0:T(8,128)(2,1)} %param.12) | copy-start | bytes 12582916
  10.0 12.9 %copy-start.8 = (f32[4096]{0:T(1024)S(1)}, f32[4096]{0:T(1024)}, u32[]{:S(2)}) copy-start(f32[4096]{0:T(1024)} %param.13) | copy-start | bytes 49156
  15.6 21.8 %all-to-all-start.2 = ((bf16[8,256,128]{2,1,0:T(8,128)(2,1)}), bf16[8,256,128]{2,1,0:T(8,128)(2,1)S(1)}, u32[]{:S(2)}, u32[]{:S(2)}) async-start(bf16[8,256,128]{2,1,0:T(8,128)(2,1)} %bitcast.11), calls=%async_computation.2 | async-start | bytes 1048576 | tf_op jit(solution)/shard_map/all_to_all | solution.py:152
  38.5 29.6 %all-to-all-start = ((bf16[8,512,128]{2,1,0:T(8,128)(2,1)}), bf16[8,512,128]{2,1,0:T(8,128)(2,1)S(1)}, u32[]{:S(2)}, u32[]{:S(2)}) async-start(bf16[8,512,128]{2,1,0:T(8,128)(2,1)} %bitcast.6), calls=%async_computation | async-start | bytes 2097152 | tf_op jit(solution)/shard_map/all_to_all | solution.py:145
  48.1 49.5 %copy-start = (f32[4]{0:T(128)S(1)}, f32[4]{0:T(128)}, u32[]{:S(2)}) copy-start(f32[4]{0:T(128)} %lam_ref.1) | copy-start | bytes 52
  48.1 49.5 %copy-start.1 = (f32[128]{0:T(128)S(1)}, f32[128]{0:T(128)}, u32[]{:S(2)}) copy-start(f32[128]{0:T(128)} %param.21) | copy-start | bytes 1540
  134.3 18.4 %all-to-all-start.3 = ((bf16[8,256,128]{2,1,0:T(8,128)(2,1)}), bf16[8,256,128]{2,1,0:T(8,128)(2,1)S(1)}, u32[]{:S(2)}, u32[]{:S(2)}) async-start(bf16[8,256,128]{2,1,0:T(8,128)(2,1)} %attend.1), calls=%async_computation.3 | async-start | bytes 1048576 | tf_op jit(solution)/shard_map/all_to_all | solution.py:178
  137.9 9.8 %copy-start.6 = (bf16[8,64,64]{2,1,0:T(8,128)(2,1)S(1)}, bf16[8,64,64]{2,1,0:T(8,128)(2,1)}, u32[]{:S(2)}) copy-start(bf16[8,64,64]{2,1,0:T(8,128)(2,1)} %param.18) | copy-start | bytes 196612
  137.9 71.0 %reduce-scatter.2.cloned.1.call-start = ((), (), s32[]{:S(2)}) async-start(), calls=%async_computation.5 | async-start | bytes 5242880 | tf_op jit(solution)/shard_map/reduce_scatter | solution.py:213
  144.0 5.2 %copy-start.5 = (bf16[512,512]{1,0:T(8,128)(2,1)}, bf16[512,512]{1,0:T(8,128)(2,1)S(1)}, u32[]{:S(2)}) copy-start(bf16[512,512]{1,0:T(8,128)(2,1)S(1)} %convolution_convert_fusion.2.x_ref) | copy-start | bytes 1572868
  144.0 5.2 %collective-permute-start = (bf16[16,512]{1,0:T(8,128)(2,1)S(1)}, bf16[16,512]{1,0:T(8,128)(2,1)S(1)}, u32[]{:S(2)}, u32[]{:S(2)}) collective-permute-start(bf16[16,512]{1,0:T(8,128)(2,1)S(1)} %slice.12), channel_id=1, source_target_pairs={{0,4},{4,8},{8,12},{12,16},{16,20},{20,24},{24,28},{1,5},{5,9},{9,... | collective-permute-start | bytes 49160 | tf_op jit(solution)/shard_map/ppermute | solution.py:203
  149.2 0.6 copy-start.7
  153.1 4.7 %copy-start.3 = (bf16[512,4096]{1,0:T(8,128)(2,1)S(1)}, bf16[512,4096]{1,0:T(8,128)(2,1)}, u32[]{:S(2)}) copy-start(bf16[512,4096]{1,0:T(8,128)(2,1)} %param.22) | copy-start | bytes 12582916
  153.1 4.7 %copy-start.4 = (bf16[512,512]{1,0:T(8,128)(2,1)S(1)}, bf16[512,512]{1,0:T(8,128)(2,1)}, u32[]{:S(2)}) copy-start(bf16[512,512]{1,0:T(8,128)(2,1)} %pooling.1) | copy-start | bytes 1572868
Sparse Core Ops, SparseCore 0:
  162.3 46.5 reduce-scatter.1
